TPU v7x, 32 devices: a whole 2x2x4 slice. The times are simulated.
32 devices in a mesh: sp: 16 (over z, y, x), tp: 2 (over core).
Axes of the slice: x: 2, y: 2, z: 4, core: 2. Of those that a mesh axis runs over, the one named last changes fastest.
Arguments:
- latent: bfloat16 [4096, 2048], P(('sp', 'tp')), may hold values from -3 to 3
- context: bfloat16 [1024, 2048], P('sp'), may hold values from -6 to 6
- condition: float32 [2048], replicated, may hold values from -6 to 6
- ctx_cond: float32 [2048], replicated, may hold values from -6 to 6
- norm_gain: float32 [2048], replicated, may hold values from 0.1 to 1.9
- w_shift: bfloat16 [2048, 2048], P('sp', 'tp'), may hold values from -0.25 to 0.25
- w_scale: bfloat16 [2048, 2048], P('sp', 'tp'), may hold values from -0.25 to 0.25
- w_gate: bfloat16 [2048, 2048], P('sp', 'tp'), may hold values from -0.25 to 0.25
- w_query: bfloat16 [2048, 2048], P(None, 'tp'), may hold values from -0.125 to 0.125
- w_key: bfloat16 [2048, 2048], P(None, 'tp'), may hold values from -0.125 to 0.125
- w_value: bfloat16 [2048, 2048], P(None, 'tp'), may hold values from -0.125 to 0.125
- w_out: bfloat16 [2048, 2048], P('tp'), may hold values from -0.125 to 0.125
- rel_bias: float32 [16, 15, 31], replicated, may hold values from 2 to 250
Outputs:
- updated: bfloat16 [4096, 2048], P(('sp', 'tp'))
All inputs are finite; a program needn't handle non-finite values.
Results may differ from a plain program's by a relative error of at most 0.015.
Values may be sent and summed in bfloat16 or wider, within the bound.
A program may use at most 128 MiB of HBM per device.

v0:
```python
import jax
import jax.numpy as jnp
from jax import lax
from jax.sharding import PartitionSpec as P

HEADS = 16
HEAD_DIM = 128
GRID_W = 32
WIN_H = 8
WIN_W = 16
NORM_EPS = 1e-06
NEG_BIG = -1e30


def padded_2(cells, sides, width):
    for axis, dim in sides:
        count = lax.axis_size(axis)
        ends = count - 1
        head = lax.slice_in_dim(cells, 0, width, axis=dim)
        tail = lax.slice_in_dim(cells, cells.shape[dim] - width, cells.shape[dim], axis=dim)
        cells = jnp.concatenate(
            [
                lax.ppermute(tail, axis, [(i, (i + 1) % count) for i in range(ends)]),
                cells,
                lax.ppermute(head, axis, [((i + 1) % count, i) for i in range(ends)]),
            ],
            axis=dim,
        )
    return cells


def rms_mod(block, norm_gain, shifts, scales):
    block = block.astype(jnp.float32)
    normed = (
        block * lax.rsqrt(jnp.mean(block * block, axis=-1, keepdims=True) + NORM_EPS) * norm_gain
    )
    return (normed * (1.0 + scales) + shifts).astype(jnp.bfloat16)


def project(block, weights):
    return jnp.stack(
        [
            jnp.dot(block, weight, preferred_element_type=jnp.float32).astype(jnp.bfloat16)
            for weight in weights
        ]
    )


def on_device(
    latent,
    context,
    condition,
    ctx_cond,
    norm_gain,
    w_shift,
    w_scale,
    w_gate,
    w_query,
    w_key,
    w_value,
    w_out,
    rel_bias,
):
    tp_size = lax.axis_size("tp")
    sp_size = lax.axis_size("sp")
    head_dev = HEADS // tp_size
    head_cols = w_query.shape[1]
    model_width = w_query.shape[0]
    row_part = w_shift.shape[0]
    col_part = w_shift.shape[1]
    activated = jax.nn.silu(jnp.stack([condition, ctx_cond])).astype(jnp.bfloat16)
    act_rows = lax.dynamic_slice_in_dim(activated, lax.axis_index("sp") * row_part, row_part, 1)
    partial_value = jnp.concatenate(
        [
            jnp.dot(act_rows, w_shift, preferred_element_type=jnp.float32),
            jnp.dot(act_rows, w_scale, preferred_element_type=jnp.float32),
            jnp.dot(act_rows[:1], w_gate, preferred_element_type=jnp.float32),
        ],
        axis=0,
    )
    placed = lax.dynamic_update_slice_in_dim(
        jnp.zeros((5, model_width), jnp.float32), partial_value, lax.axis_index("tp") * col_part, 1
    )
    mod_vecs = lax.psum(placed, ("sp", "tp"))
    normed = rms_mod(latent, norm_gain, mod_vecs[0], mod_vecs[2])
    projected = project(lax.all_gather(normed, "tp", axis=0, tiled=True), (w_query, w_key, w_value))
    ctx_kv = lax.all_gather(
        project(rms_mod(context, norm_gain, mod_vecs[1], mod_vecs[3]), (w_key, w_value)),
        "sp",
        axis=1,
        tiled=True,
    )
    ctx_key3 = ctx_kv[0].reshape(-1, head_dev, HEAD_DIM)
    ctx_val3 = ctx_kv[1].reshape(-1, head_dev, HEAD_DIM)
    grid_rows = projected.shape[1] // GRID_W
    queries = projected[0].reshape(grid_rows, GRID_W, head_dev, HEAD_DIM)
    half_win = WIN_H // 2
    padded = padded_2(
        projected[1:].reshape(2, grid_rows, GRID_W, head_cols), (("sp", 1),), half_win
    )
    total_rows = grid_rows * sp_size
    first_row = lax.axis_index("sp") * grid_rows
    local_rows = jnp.arange(grid_rows, dtype=jnp.int32)
    starts = (
        jnp.clip(first_row + local_rows - half_win, 0, total_rows - WIN_H) - first_row + half_win
    )

    def take_window(start_row):
        return lax.dynamic_slice_in_dim(padded, start_row, WIN_H, 1)

    windows = jax.vmap(take_window)(starts)
    key_win = windows[:, 0].reshape(grid_rows, WIN_H, GRID_W, head_dev, HEAD_DIM)
    val_win = windows[:, 1].reshape(grid_rows, WIN_H, GRID_W, head_dev, HEAD_DIM)
    row_off = (
        starts[:, None]
        - half_win
        + jnp.arange(WIN_H, dtype=jnp.int32)[None, :]
        - local_rows[:, None]
        + WIN_H
        - 1
    )
    col_ids = jnp.arange(GRID_W, dtype=jnp.int32)
    col_start = jnp.clip(col_ids - WIN_W // 2, 0, GRID_W - WIN_W)
    col_in = (col_ids[None, :] >= col_start[:, None]) & (
        col_ids[None, :] < col_start[:, None] + WIN_W
    )
    col_off = jnp.clip(col_ids[None, :] - col_ids[:, None], 1 - WIN_W, WIN_W - 1) + WIN_W - 1
    col_hot = (col_off[:, :, None] == jnp.arange(2 * WIN_W - 1)[None, None, :]).astype(jnp.float32)
    row_hot = (row_off[:, :, None] == jnp.arange(2 * WIN_H - 1)[None, None, :]).astype(jnp.float32)
    bias_table = lax.dynamic_slice_in_dim(rel_bias, lax.axis_index("tp") * head_dev, head_dev, 0)
    col_table = jnp.einsum("hec,qwc->heqw", bias_table, col_hot, precision=lax.Precision.HIGHEST)
    bias_win = jnp.einsum("rke,heqw->rqhkw", row_hot, col_table, precision=lax.Precision.HIGHEST)
    inv_scale = HEAD_DIM ** (-0.5)
    scores_win = (
        jnp.einsum("rqhd,rkwhd->rqhkw", queries, key_win, preferred_element_type=jnp.float32)
        * inv_scale
        + bias_win
    )
    scores_win = jnp.where(col_in[None, :, None, None, :], scores_win, NEG_BIG)
    scores_win = scores_win.reshape(grid_rows, GRID_W, head_dev, WIN_H * GRID_W)
    scores_ctx = (
        jnp.einsum("rqhd,chd->rqhc", queries, ctx_key3, preferred_element_type=jnp.float32)
        * inv_scale
    )
    row_max = jnp.maximum(jnp.max(scores_win, axis=-1), jnp.max(scores_ctx, axis=-1))
    exp_win = jnp.exp(scores_win - row_max[..., None])
    exp_ctx = jnp.exp(scores_ctx - row_max[..., None])
    row_total = jnp.sum(exp_win, axis=-1) + jnp.sum(exp_ctx, axis=-1)
    probs_win = (exp_win / row_total[..., None]).astype(jnp.bfloat16)
    probs_win = probs_win.reshape(grid_rows, GRID_W, head_dev, WIN_H, GRID_W)
    probs_ctx = (exp_ctx / row_total[..., None]).astype(jnp.bfloat16)
    attended = jnp.einsum(
        "rqhkw,rkwhd->rqhd", probs_win, val_win, preferred_element_type=jnp.float32
    )
    attended = attended + jnp.einsum(
        "rqhc,chd->rqhd", probs_ctx, ctx_val3, preferred_element_type=jnp.float32
    )
    attended = attended.astype(jnp.bfloat16).reshape(grid_rows * GRID_W, head_cols)
    branch = lax.psum_scatter(
        jnp.dot(attended, w_out, preferred_element_type=jnp.float32).astype(jnp.bfloat16),
        "tp",
        scatter_dimension=0,
        tiled=True,
    ).astype(jnp.float32)
    return (latent.astype(jnp.float32) + mod_vecs[4] * branch).astype(jnp.bfloat16)


def solution(mesh):
    placed = (
        P(("sp", "tp"), None),
        P("sp", None),
        P(),
        P(),
        P(),
        P("sp", "tp"),
        P("sp", "tp"),
        P("sp", "tp"),
        P(None, "tp"),
        P(None, "tp"),
        P(None, "tp"),
        P("tp", None),
        P(),
    )
    return jax.shard_map(
        on_device, mesh=mesh, in_specs=placed, out_specs=P(("sp", "tp"), None), check_vma=False
    )
```

profile of v0, /device:TPU:0, one launch (start us, length us, event | category | flops | bytes accessed | tf_op | source)
XLA Modules:
  0.0 193.7 jit_solution(12751256618278326930)
XLA Ops:
  6.6 0.8 fusion.61
  7.4 0.2 copy-done
  7.5 0.1 fusion.69
  7.7 1.1 fusion.70
  8.8 1.1 fusion.63
  9.9 42.3 %psum.7 = f32[5,2048]{1,0:T(8,128)S(1)} all-reduce(f32[5,2048]{1,0:T(8,128)S(1)} %maximum_dynamic-update-slice_fusion), channel_id=1, replica_groups=mesh['sp'=16,'tp'=2] {'sp','tp'}, use_global_device_ids=true, to_apply=%region_0.1 | all-reduce | flops 10240 | bytes 81920 | tf_op jit(solution)/shard_map/psum | solution.py:84
  52.2 1.2 fusion.35
  53.5 2.1 %fusion.39 = bf16[128,2048]{1,0:T(8,128)(2,1)} fusion(bf16[128,2048]{1,0:T(8,128)(2,1)} %param.13, f32[2048]{0:T(1024)S(1)} %bitcast.155, f32[2048]{0:T(1024)S(1)} %bitcast.156, f32[2048]{0:T(1024)} %param.17, f32[128]{0:T(128)S(1)} %add_rsqrt_fusion.1), kind=kLoop, calls=%fused_computation.46 | loop fusion | flops 1572864 | bytes 1073664 | tf_op jit(solution)/shard_map/convert_element_type | solution.py:37
  55.6 0.0 all-gather.3.cloned.1.call-update
  55.6 0.0 all-gather.5.cloned.1.call-start
  55.7 0.0 copy-start.3
  55.7 1.3 fusion.41
  56.9 0.0 copy-start.8
  57.0 3.2 %fusion.33 = bf16[1,64,1024]{2,1,0:T(8,128)(2,1)S(1)} fusion(bf16[2048,1024]{1,0:T(8,128)(2,1)} %param.22, bf16[64,2048]{1,0:T(8,128)(2,1)} %param.14, f32[2048]{0:T(1024)S(1)} %bitcast.150, f32[2048]{0:T(1024)S(1)} %bitcast.152, f32[2048]{0:T(1024)} %param.17, f32[64]{0:T(128)S(1)} %add_rsqrt_fusion), kind=kOutput, calls=%fused_computation.40 | convolution fusion | flops 269287424 | bytes 4612352 | tf_op jit(solution)/shard_map/dot_general | solution.py:43
  60.2 0.9 fusion.34
  61.1 0.7 pad_maximum_fusion.2
  61.9 0.0 all-gather.5.cloned.1.call-update
  61.9 0.0 reduce-scatter.2.cloned.1.call-start
  62.0 0.1 subtract_add_fusion
  62.1 1.4 fusion.51
  63.5 5.6 %fusion.12 = f32[8,32,32,8,8]{2,4,3,1,0:T(8,128)} fusion(f32[8,15,32,32]{3,1,2,0:T(8,128)S(1)} %fusion.51, s32[8,8]{1,0:T(8,128)S(1)} %subtract_add_fusion), kind=kOutput, calls=%fused_computation.21 | convolution fusion | flops 94372800 | bytes 2588928 | tf_op jit(solution)/shard_map/rke,heqw->rqhkw/dot_general | solution.py:132
  69.2 9.3 %copy.59 = f32[8,32,32,8,8]{1,2,4,0,3:T(8,128)} copy(f32[8,32,32,8,8]{2,4,3,1,0:T(8,128)} %fusion.12) | data formatting | bytes 4194304 | tf_op jit(solution)/shard_map/rke,heqw->rqhkw/dot_general | solution.py:132
  78.5 0.0 all-gather.3.cloned.1.call-done
  78.5 0.0 copy-start.4
  78.5 3.9 %convolution_convert_fusion.2 = bf16[256,1024]{1,0:T(8,128)(2,1)S(1)} fusion(bf16[256,2048]{1,0:T(8,128)(2,1)} %all-gather.3.cloned.1.call-done, bf16[2048,1024]{1,0:T(8,128)(2,1)} %param.23), kind=kOutput, calls=%fused_computation.35 | convolution fusion | flops 1074003968 | bytes 5767168 | tf_op jit(solution)/shard_map/dot_general | solution.py:43
  82.4 0.1 copy-done.10
  82.6 1.3 convolution_convert_fusion.3
  83.8 0.1 fusion.46
  83.9 4.2 %collective-permute-start = (bf16[2,4,32,1024]{3,2,0,1:T(8,128)(2,1)S(1)}, bf16[2,4,32,1024]{3,2,0,1:T(8,128)(2,1)S(1)}, u32[]{:S(2)}, u32[]{:S(2)}) collective-permute-start(bf16[2,4,32,1024]{3,2,0,1:T(8,128)(2,1)S(1)} %get-tuple-element.9), channel_id=1, source_target_pairs={{0,2},{2,4},{4,6},{6,8},{8,10},{10,12},{12,14},{14,16},{16,18},{18... | collective-permute-start | bytes 1572872 | tf_op jit(solution)/shard_map/ppermute | solution.py:23
  88.2 1.3 collective-permute-start.1
  89.5 1.3 fusion.32
  90.8 0.1 copy.82
  90.9 0.1 copy.61
  91.0 25.2 %collective-permute-done = bf16[2,4,32,1024]{3,2,0,1:T(8,128)(2,1)S(1)} collective-permute-done((bf16[2,4,32,1024]{3,2,0,1:T(8,128)(2,1)S(1)}, bf16[2,4,32,1024]{3,2,0,1:T(8,128)(2,1)S(1)}, u32[]{:S(2)}, u32[]{:S(2)}) %collective-permute-start) | collective-permute-done | bytes 524320 | tf_op jit(solution)/shard_map/ppermute | solution.py:23
  116.2 1.9 collective-permute-done.1
  118.1 0.3 pad_maximum_fusion
  118.4 4.9 %gather_fusion = bf16[8,2,8,32,1024]{4,3,1,2,0:T(8,128)(2,1)} fusion(bf16[2,16,32,1024]{3,2,0,1:T(8,128)(2,1)S(1)} %pad_maximum_fusion, s32[8]{0:T(128)S(1)} %shift-left_bitcast_fusion), kind=kCustom, calls=%fused_computation | custom fusion | bytes 16777344 | tf_op jit(solution)/shard_map/vmap()/gather | solution.py:109
  123.3 4.0 %fusion.66 = (bf16[8,1,8,32,1024]{4,3,1,2,0:T(8,128)(2,1)S(1)}, bf16[8,1,8,32,1024]{4,3,1,2,0:T(8,128)(2,1)S(1)}) fusion(bf16[8,2,8,32,1024]{4,3,1,2,0:T(8,128)(2,1)} %gather_fusion), kind=kLoop, calls=%fused_computation.99 | loop fusion | bytes 16777216 | tf_op jit(solution)/shard_map/slice | solution.py:113
  127.3 0.0 slice-start
  127.3 1.1 copy.81
  128.4 0.0 slice-start.1
  128.4 3.3 %copy.80 = bf16[256,8,8,128]{3,2,1,0:T(8,128)(2,1)} copy(bf16[256,8,8,128]{3,1,2,0:T(8,128)(2,1)S(1)} %bitcast.137) | data formatting | bytes 8388608
  131.7 1.2 slice-done.1
  132.9 4.3 %fusion.68 = (f32[8,32,8]{1,2,0:T(8,128)S(1)}, f32[8,32,8,8,32]{1,4,3,2,0:T(8,128)}) fusion(f32[8,32,32,8,8]{1,2,4,0,3:T(8,128)S(1)} %bitcast.133, bf16[8,32,8,128,1]{3,2,1,0,4:T(8,128)(2,1)S(1)} %bitcast_bitcast_fusion, bf16[8,8,32,8,128]{4,3,2,1,0:T(8,128)(2,1)S(1)} %bitcast.136, pred[32,32]{0,1:T(8,128)(4,1)S(1)} %fusion.57), kind=kOutput, calls=%fused_computation.101 | convolution fusion | flops 136312832 | bytes 8922112 | tf_op jit(solution)/shard_map/rqhd,rkwhd->rqhkw/dot_general | solution.py:135
  137.2 19.0 %all-gather.5.cloned.1.call-done = bf16[2,1024,1024]{2,1,0:T(8,128)(2,1)} async-done(((bf16[2,64,1024]{2,1,0:T(8,128)(2,1)}), bf16[2,1024,1024]{2,1,0:T(8,128)(2,1)}) %all-gather.5.cloned.1.call-update) | async-done | bytes 4194320 | tf_op jit(solution)/shard_map/all_gather | solution.py:87
  156.2 3.2 %slice_bitcast_fusion = (bf16[128,8,8,128]{3,1,2,0:T(8,128)(2,1)S(1)}, bf16[128,8,8,128]{3,1,2,0:T(8,128)(2,1)S(1)}) fusion(bf16[2,1024,1024]{2,1,0:T(8,128)(2,1)} %all-gather.5.cloned.1.call-done), kind=kLoop, calls=%fused_computation.18 | loop fusion | bytes 8388608
  159.4 0.6 copy.83
  160.0 1.3 fusion.16
  161.3 0.0 slice-start.2
  161.3 0.7 bitcast_reduce_fusion
  162.0 0.0 slice-start.3
  162.0 1.9 fusion.3
  163.9 1.0 slice-done.3
  164.9 2.0 %fusion.2 = f32[8,32,8]{1,2,0:T(8,128)S(1)} fusion(f32[8,32,8,8,32]{1,4,3,2,0:T(8,128)S(1)} %bitcast.135, f32[8,32,8]{1,2,0:T(8,128)S(1)} %copy_maximum_fusion), kind=kLoop, calls=%fused_computation.9 | loop fusion | flops 1046528 | bytes 2113536 | tf_op jit(solution)/shard_map/reduce_sum | solution.py:148
  167.0 0.6 copy.84
  167.6 3.3 %fusion.21 = f32[8,32,8,128]{3,1,2,0:T(8,128)S(1)} fusion(bf16[1024,8,128]{2,1,0:T(8,128)(2,1)S(1)} %bitcast.143, f32[8,32,8]{1,0,2:T(8,128)S(1)} %copy.67, f32[8,32,8]{1,0,2:T(8,128)S(1)} %copy.63, f32[8,1024,256]{1,2,0:S(1)} %fusion.16), kind=kOutput, calls=%fused_computation.31 | convolution fusion | flops 545259520 | bytes 11550720 | tf_op jit(solution)/shard_map/rqhc,chd->rqhd/dot_general | solution.py:155
  170.9 2.3 %fusion.29 = bf16[8,32,8,128]{3,1,2,0:T(8,128)(2,1)S(1)} fusion(f32[8,32,8,128]{3,1,2,0:T(8,128)S(1)} %fusion.21, f32[8,32,8,8,32]{1,4,3,2,0:T(8,128)S(1)} %bitcast.135, f32[8,32,8]{1,2,0:T(8,128)S(1)} %copy_add_fusion, f32[8,32,8]{1,2,0:T(8,128)S(1)} %copy_maximum_fusion, bf16[8,8,32,8,128]{4,3,2,1,0:T(8,128)(2,1)S(1)} %bitcast.142), kind=kOutput, calls=%fused_computation.33 | convolution fusion | flops 136314880 | bytes 7880704 | tf_op jit(solution)/shard_map/rqhkw,rkwhd->rqhd/dot_general | solution.py:152
  173.2 0.2 copy.70
  173.5 0.0 copy-start.2
  173.5 0.0 copy-start.1
  173.5 4.5 %convolution_convert_fusion = bf16[256,2048]{1,0:T(8,128)(2,1)} fusion(bf16[1024,2048]{1,0:T(8,128)(2,1)} %param.24, bf16[32,8,8,128]{3,2,1,0:T(8,128)(2,1)S(1)} %bitcast.149), kind=kOutput, calls=%fused_computation.17 | convolution fusion | flops 1074266112 | bytes 5767168 | tf_op jit(solution)/shard_map/dot_general | solution.py:160
  178.0 0.0 reduce-scatter.2.cloned.1.call-update
  178.0 7.1 %reduce-scatter.2.cloned.1.call-done = bf16[128,2048]{1,0:T(8,128)(2,1)} async-done(((bf16[256,2048]{1,0:T(8,128)(2,1)}), bf16[128,2048]{1,0:T(8,128)(2,1)}) %reduce-scatter.2.cloned.1.call-update) | async-done | bytes 524304 | tf_op jit(solution)/shard_map/reduce_scatter | solution.py:159
  185.1 2.0 %fusion.40 = bf16[128,2048]{1,0:T(8,128)(2,1)} fusion(bf16[128,2048]{1,0:T(8,128)(2,1)S(1)} %copy-done.2, bf16[128,2048]{1,0:T(8,128)(2,1)} %reduce-scatter.2.cloned.1.call-done, f32[2048]{0:T(1024)S(1)} %bitcast.154), kind=kLoop, calls=%fused_computation.47 | loop fusion | flops 1310720 | bytes 1581056 | tf_op jit(solution)/shard_map/convert_element_type | solution.py:165
  (36 shorter events, 0.2 us)
Async XLA Ops:
  6.5 1.0 copy-start
  6.5 53.7 %copy-start.7 = (f32[2048]{0:T(1024)S(1)}, f32[2048]{0:T(1024)}, u32[]{:S(2)}) copy-start(f32[2048]{0:T(1024)} %param.17) | copy-start | bytes 24580
  6.5 53.7 %copy-start.6 = (bf16[64,2048]{1,0:T(8,128)(2,1)S(1)}, bf16[64,2048]{1,0:T(8,128)(2,1)}, u32[]{:S(2)}) copy-start(bf16[64,2048]{1,0:T(8,128)(2,1)} %param.14) | copy-start | bytes 786436
  6.5 72.0 %all-gather.3.cloned.1.call-start = ((), (), s32[]{:S(2)}) async-start(), calls=%async_computation.1 | async-start | bytes 1572864 | tf_op jit(solution)/shard_map/all_gather | solution.py:86
  55.6 100.6 %all-gather.5.cloned.1.call-start = ((), (), s32[]{:S(2)}) async-start(), calls=%async_computation.2 | async-start | bytes 4456448 | tf_op jit(solution)/shard_map/all_gather | solution.py:87
  55.7 4.6 %copy-start.3 = (bf16[2048,1024]{1,0:T(8,128)(2,1)S(1)}, bf16[2048,1024]{1,0:T(8,128)(2,1)}, u32[]{:S(2)}) copy-start(bf16[2048,1024]{1,0:T(8,128)(2,1)} %param.23) | copy-start | bytes 12582916
  56.9 5.0 %copy-start.8 = (f32[16,15,31]{2,0,1:T(8,128)S(1)}, f32[16,15,31]{2,0,1:T(8,128)}, u32[]{:S(2)}) copy-start(f32[16,15,31]{2,0,1:T(8,128)} %param.25) | copy-start | bytes 89284
  61.9 123.2 %reduce-scatter.2.cloned.1.call-start = ((), (), s32[]{:S(2)}) async-start(), calls=%async_computation.3 | async-start | bytes 1572864 | tf_op jit(solution)/shard_map/reduce_scatter | solution.py:159
  78.5 3.9 %copy-start.4 = (bf16[2048,1024]{1,0:T(8,128)(2,1)S(1)}, bf16[2048,1024]{1,0:T(8,128)(2,1)}, u32[]{:S(2)}) copy-start(bf16[2048,1024]{1,0:T(8,128)(2,1)} %param.22) | copy-start | bytes 12582916
  78.5 4.0 %copy-start.10 = (bf16[256,2048]{1,0:T(8,128)(2,1)S(1)}, bf16[256,2048]{1,0:T(8,128)(2,1)}, u32[]{:S(2)}) copy-start(bf16[256,2048]{1,0:T(8,128)(2,1)} %all-gather.3.cloned.1.call-done) | copy-start | bytes 3145732
  82.6 6.9 %copy-start.9 = (bf16[2048,1024]{1,0:T(8,128)(2,1)S(1)}, bf16[2048,1024]{1,0:T(8,128)(2,1)}, u32[]{:S(2)}) copy-start(bf16[2048,1024]{1,0:T(8,128)(2,1)} %param.21) | copy-start | bytes 12582916
  83.9 32.3 %collective-permute-start = (bf16[2,4,32,1024]{3,2,0,1:T(8,128)(2,1)S(1)}, bf16[2,4,32,1024]{3,2,0,1:T(8,128)(2,1)S(1)}, u32[]{:S(2)}, u32[]{:S(2)}) collective-permute-start(bf16[2,4,32,1024]{3,2,0,1:T(8,128)(2,1)S(1)} %get-tuple-element.9), channel_id=1, source_target_pairs={{0,2},{2,4},{4,6},{6,8},{8,10},{10,12},{12,14},{14,16},{16,18},{18... | collective-permute-start | bytes 1572872 | tf_op jit(solution)/shard_map/ppermute | solution.py:23
  88.2 30.0 %collective-permute-start.1 = (bf16[2,4,32,1024]{3,2,0,1:T(8,128)(2,1)S(1)}, bf16[2,4,32,1024]{3,2,0,1:T(8,128)(2,1)S(1)}, u32[]{:S(2)}, u32[]{:S(2)}) collective-permute-start(bf16[2,4,32,1024]{3,2,0,1:T(8,128)(2,1)S(1)} %get-tuple-element.10), channel_id=1, source_target_pairs={{2,0},{4,2},{6,4},{8,6},{10,8},{12,10},{14,12},{16,14},{18,16},{20... | collective-permute-start | bytes 1572872 | tf_op jit(solution)/shard_map/ppermute | solution.py:25
  127.3 4.5 %slice-start = ((s8[8388608]{0:T(1024)(128)(4,1)}), s8[4194304]{0:T(1024)(128)(4,1)S(1)}, s32[]{:S(2)}) async-start(s8[8388608]{0:T(1024)(128)(4,1)} %bitcast.132), calls=%async_computation.4 | async-start | bytes 8388608
  128.4 4.5 %slice-start.1 = ((s8[8388608]{0:T(1024)(128)(4,1)}), s8[4194304]{0:T(1024)(128)(4,1)S(1)}, s32[]{:S(2)}) async-start(s8[8388608]{0:T(1024)(128)(4,1)} %bitcast.132), calls=%async_computation.5 | async-start | bytes 8388608
  161.3 2.6 %slice-start.2 = ((s8[8388608]{0:T(1024)(128)(4,1)}), s8[4194304]{0:T(1024)(128)(4,1)S(1)}, s32[]{:S(2)}) async-start(s8[8388608]{0:T(1024)(128)(4,1)} %bitcast.134), calls=%async_computation.6 | async-start | bytes 8388608
  162.0 2.9 %slice-start.3 = ((s8[8388608]{0:T(1024)(128)(4,1)}), s8[4194304]{0:T(1024)(128)(4,1)S(1)}, s32[]{:S(2)}) async-start(s8[8388608]{0:T(1024)(128)(4,1)} %bitcast.134), calls=%async_computation.7 | async-start | bytes 8388608
  167.6 3.3 %copy-start.5 = (bf16[256,8,8,128]{3,2,1,0:T(8,128)(2,1)S(1)}, bf16[256,8,8,128]{3,2,1,0:T(8,128)(2,1)}, u32[]{:S(2)}) copy-start(bf16[256,8,8,128]{3,2,1,0:T(8,128)(2,1)} %copy.80) | copy-start | bytes 12582916
  173.5 11.7 %copy-start.2 = (bf16[128,2048]{1,0:T(8,128)(2,1)S(1)}, bf16[128,2048]{1,0:T(8,128)(2,1)}, u32[]{:S(2)}) copy-start(bf16[128,2048]{1,0:T(8,128)(2,1)} %param.13) | copy-start | bytes 1572868
  173.5 13.6 %copy-start.1 = (bf16[128,1024]{1,0:T(8,128)(2,1)S(1)}, bf16[128,1024]{1,0:T(8,128)(2,1)}, u32[]{:S(2)}) copy-start(bf16[128,1024]{1,0:T(8,128)(2,1)} %param.18) | copy-start | bytes 786436
Sparse Core Ops, SparseCore 0:
  55.7 8.8 all-gather.2
  67.3 88.8 all-gather.4
  178.1 6.9 reduce-scatter.1
where the time goes:
time: 194 us
  waiting for transfers between devices  53.3 us (27%)
  blocking collectives  42.3 us (22%)
  matrix products  35.6 us (18%)
  local copies, waits for them, and re-layouts  30 us (15%)
  between operations  13.6 us (7%)
  other arithmetic  13.3 us (7%)
  starting transfers between devices  5.61 us (3%)
    psum x1, blocking collectives, on_device(): mod_vecs = lax.psum(placed, ('sp', 'tp'))  42.3 us
    ppermute x1, waiting for transfers between devices, padded_2(): lax.ppermute(tail, axis, [(i, (i + 1) % count) for i in range(ends)])  25.2 us
    all_gather x1, waiting for transfers between devices, on_device(): lax.all_gather(project(rms_mod(context, norm_gain, mod_vecs[1], mod_vecs[...  19 us
    unnamed x36, local copies, waits for them, and re-layouts  11.5 us
    dot_general x5, matrix products, project(): jnp.dot(block, weight, preferred_element_type=jnp.float32)  10.6 us
    dot_general x1, local copies, waits for them, and re-layouts, on_device(): jnp.einsum('rke,heqw->rqhkw', row_hot, col_table, precision=lax.Precision...  9.27 us
    reduce_scatter x1, waiting for transfers between devices, on_device(): lax.psum_scatter(jnp.dot(attended, w_out, preferred_element_type=jnp.floa...  7.12 us
    dot_general x1, matrix products, on_device(): jnp.einsum('rke,heqw->rqhkw', row_hot, col_table, precision=lax.Precision...  5.61 us
  transfers between devices with their start and end apart: 5, of which 4 were waited for; matrix products, arithmetic and copies ran while one was open for 24% of the time, Pallas kernels for 0%

commit v1 on v0

--- a/solution.py
+++ b/solution.py
@@ -10,6 +10,7 @@
 WIN_W = 16
 NORM_EPS = 1e-06
 NEG_BIG = -1e30
+_start_sources_all = lambda in_array: jax.lax.psum(jax.lax.psum(in_array, axis_name="sp"), "tp")
 
 
 def padded_2(cells, sides, width):
@@ -81,7 +82,7 @@
     placed = lax.dynamic_update_slice_in_dim(
         jnp.zeros((5, model_width), jnp.float32), partial_value, lax.axis_index("tp") * col_part, 1
     )
-    mod_vecs = lax.psum(placed, ("sp", "tp"))
+    mod_vecs = _start_sources_all(placed)
     normed = rms_mod(latent, norm_gain, mod_vecs[0], mod_vecs[2])
     projected = project(lax.all_gather(normed, "tp", axis=0, tiled=True), (w_query, w_key, w_value))
     ctx_kv = lax.all_gather(

time: 194 us -> 230 us (1.19)
  blocking collectives: 42.3 us -> 82.2 us
  starting transfers between devices: 5.61 us -> 2.7 us
    psum x1 -> x2, blocking collectives: 42.3 us -> 82.2 us  [the longest x1 78.7 us: jax.lax.psum(in_array, axis_name='sp')]
    ppermute x1, starting transfers between devices: 4.23 us -> 1.32 us  [padded_2(): lax.ppermute(tail, axis, [(i, (i + 1) % count) for i in range(ends)])]
    ppermute x1, waiting for transfers between devices: 25.2 us -> 27.7 us  [padded_2(): lax.ppermute(tail, axis, [(i, (i + 1) % count) for i in range(ends)])]
  transfers between devices with their start and end apart: 5 -> 5, of which waited for: 4 -> 3; matrix products, arithmetic and copies ran while one was open for 24% -> 21% of each run, Pallas kernels for 0% -> 0%
where the time goes in v1:
time: 230 us
  blocking collectives  82.2 us (36%)
  waiting for transfers between devices  52.7 us (23%)
  matrix products  36 us (16%)
  local copies, waits for them, and re-layouts  29.1 us (13%)
  between operations  13.6 us (6%)
  other arithmetic  13.3 us (6%)
  starting transfers between devices  2.7 us (1%)
    psum x1, blocking collectives, jax.lax.psum(in_array, axis_name='sp')  78.7 us
    ppermute x1, waiting for transfers between devices, padded_2(): lax.ppermute(tail, axis, [(i, (i + 1) % count) for i in range(ends)])  27.7 us
    all_gather x1, waiting for transfers between devices, on_device(): lax.all_gather(project(rms_mod(context, norm_gain, mod_vecs[1], mod_vecs[...  17.8 us
    dot_general x5, matrix products, project(): jnp.dot(block, weight, preferred_element_type=jnp.float32)  10.9 us
    unnamed x36, local copies, waits for them, and re-layouts  10.1 us
    dot_general x1, local copies, waits for them, and re-layouts, on_device(): jnp.einsum('rke,heqw->rqhkw', row_hot, col_table, precision=lax.Precision...  9.27 us
    reduce_scatter x1, waiting for transfers between devices, on_device(): lax.psum_scatter(jnp.dot(attended, w_out, preferred_element_type=jnp.floa...  7.12 us
    dot_general x1, matrix products, on_device(): jnp.einsum('rke,heqw->rqhkw', row_hot, col_table, precision=lax.Precision...  5.63 us
  transfers between devices with their start and end apart: 5, of which 3 were waited for; matrix products, arithmetic and copies ran while one was open for 21% of the time, Pallas kernels for 0%

profile of v1, /device:TPU:0, one launch (start us, length us, event | category | flops | bytes accessed | tf_op | source)
XLA Modules:
  0.0 229.7 jit_solution(7250962571477158795)
XLA Ops:
  6.6 0.8 fusion.61
  7.4 0.2 copy-done
  7.5 0.1 fusion.69
  7.7 1.1 fusion.70
  8.8 1.1 fusion.63
  9.9 78.7 %psum.14 = f32[5,2048]{1,0:T(8,128)S(1)} all-reduce(f32[5,2048]{1,0:T(8,128)S(1)} %maximum_dynamic-update-slice_fusion), channel_id=1, replica_groups=mesh['sp'=16,'tp'=2] {'sp'}, use_global_device_ids=true, to_apply=%region_0.1 | all-reduce | flops 10240 | bytes 81920 | tf_op jit(solution)/shard_map/psum | solution.py:13
  88.6 3.6 %psum.15 = f32[5,2048]{1,0:T(8,128)S(1)} all-reduce(f32[5,2048]{1,0:T(8,128)S(1)} %psum.14), channel_id=1, replica_groups=mesh['sp'=16,'tp'=2] {'tp'}, use_global_device_ids=true, to_apply=%region_1.2 | all-reduce | flops 10240 | bytes 81920 | tf_op jit(solution)/shard_map/psum | solution.py:13
  92.2 1.2 fusion.35
  93.4 2.1 fusion.39
  95.5 0.0 all-gather.3.cloned.1.call-update
  95.6 0.0 all-gather.5.cloned.1.call-start
  95.6 0.0 copy-start.3
  95.6 1.3 fusion.41
  96.9 0.0 copy-start.8
  96.9 3.6 %fusion.33 = bf16[1,64,1024]{2,1,0:T(8,128)(2,1)S(1)} fusion(bf16[2048,1024]{1,0:T(8,128)(2,1)} %param.22, bf16[64,2048]{1,0:T(8,128)(2,1)} %param.14, f32[2048]{0:T(1024)S(1)} %bitcast.150, f32[2048]{0:T(1024)S(1)} %bitcast.152, f32[2048]{0:T(1024)} %param.17, f32[64]{0:T(128)S(1)} %add_rsqrt_fusion), kind=kOutput, calls=%fused_computation.40 | convolution fusion | flops 269287424 | bytes 4612352 | tf_op jit(solution)/shard_map/dot_general | solution.py:44
  100.5 0.9 fusion.34
  101.4 0.7 pad_maximum_fusion.2
  102.2 0.0 all-gather.5.cloned.1.call-update
  102.2 0.0 reduce-scatter.2.cloned.1.call-start
  102.3 0.1 subtract_add_fusion
  102.4 1.4 fusion.51
  103.8 5.6 %fusion.12 = f32[8,32,32,8,8]{2,4,3,1,0:T(8,128)} fusion(f32[8,15,32,32]{3,1,2,0:T(8,128)S(1)} %fusion.51, s32[8,8]{1,0:T(8,128)S(1)} %subtract_add_fusion), kind=kOutput, calls=%fused_computation.21 | convolution fusion | flops 94372800 | bytes 2588928 | tf_op jit(solution)/shard_map/rke,heqw->rqhkw/dot_general | solution.py:133
  109.5 9.3 %copy.59 = f32[8,32,32,8,8]{1,2,4,0,3:T(8,128)} copy(f32[8,32,32,8,8]{2,4,3,1,0:T(8,128)} %fusion.12) | data formatting | bytes 4194304 | tf_op jit(solution)/shard_map/rke,heqw->rqhkw/dot_general | solution.py:133
  118.8 0.0 all-gather.3.cloned.1.call-done
  118.8 0.0 copy-start.4
  118.8 3.9 %convolution_convert_fusion.2 = bf16[256,1024]{1,0:T(8,128)(2,1)S(1)} fusion(bf16[256,2048]{1,0:T(8,128)(2,1)} %all-gather.3.cloned.1.call-done, bf16[2048,1024]{1,0:T(8,128)(2,1)} %param.23), kind=kOutput, calls=%fused_computation.35 | convolution fusion | flops 1074003968 | bytes 5767168 | tf_op jit(solution)/shard_map/dot_general | solution.py:44
  122.7 0.1 copy-done.10
  122.9 1.3 convolution_convert_fusion.3
  124.1 0.1 fusion.46
  124.2 1.3 collective-permute-start
  125.6 1.3 collective-permute-start.1
  126.9 1.3 fusion.32
  128.2 0.1 copy.82
  128.3 0.1 copy.61
  128.4 27.7 %collective-permute-done = bf16[2,4,32,1024]{3,2,0,1:T(8,128)(2,1)S(1)} collective-permute-done((bf16[2,4,32,1024]{3,2,0,1:T(8,128)(2,1)S(1)}, bf16[2,4,32,1024]{3,2,0,1:T(8,128)(2,1)S(1)}, u32[]{:S(2)}, u32[]{:S(2)}) %collective-permute-start) | collective-permute-done | bytes 524320 | tf_op jit(solution)/shard_map/ppermute | solution.py:24
  156.1 0.0 collective-permute-done.1
  156.1 0.3 pad_maximum_fusion
  156.4 4.9 %gather_fusion = bf16[8,2,8,32,1024]{4,3,1,2,0:T(8,128)(2,1)} fusion(bf16[2,16,32,1024]{3,2,0,1:T(8,128)(2,1)S(1)} %pad_maximum_fusion, s32[8]{0:T(128)S(1)} %shift-left_bitcast_fusion), kind=kCustom, calls=%fused_computation | custom fusion | bytes 16777344 | tf_op jit(solution)/shard_map/vmap()/gather | solution.py:110
  161.3 4.5 %fusion.66 = (bf16[8,1,8,32,1024]{4,3,1,2,0:T(8,128)(2,1)S(1)}, bf16[8,1,8,32,1024]{4,3,1,2,0:T(8,128)(2,1)S(1)}) fusion(bf16[8,2,8,32,1024]{4,3,1,2,0:T(8,128)(2,1)} %gather_fusion), kind=kLoop, calls=%fused_computation.99 | loop fusion | bytes 16777216 | tf_op jit(solution)/shard_map/slice | solution.py:114
  165.8 0.0 slice-start
  165.8 1.1 copy.81
  166.9 0.0 slice-start.1
  167.0 3.1 %copy.80 = bf16[256,8,8,128]{3,2,1,0:T(8,128)(2,1)} copy(bf16[256,8,8,128]{3,1,2,0:T(8,128)(2,1)S(1)} %bitcast.137) | data formatting | bytes 8388608
  170.1 4.3 %fusion.68 = (f32[8,32,8]{1,2,0:T(8,128)S(1)}, f32[8,32,8,8,32]{1,4,3,2,0:T(8,128)}) fusion(f32[8,32,32,8,8]{1,2,4,0,3:T(8,128)S(1)} %bitcast.133, bf16[8,32,8,128,1]{3,2,1,0,4:T(8,128)(2,1)S(1)} %bitcast_bitcast_fusion, bf16[8,8,32,8,128]{4,3,2,1,0:T(8,128)(2,1)S(1)} %bitcast.136, pred[32,32]{0,1:T(8,128)(4,1)S(1)} %fusion.57), kind=kOutput, calls=%fused_computation.101 | convolution fusion | flops 136312832 | bytes 8922112 | tf_op jit(solution)/shard_map/rqhd,rkwhd->rqhkw/dot_general | solution.py:136
  174.4 17.8 %all-gather.5.cloned.1.call-done = bf16[2,1024,1024]{2,1,0:T(8,128)(2,1)} async-done(((bf16[2,64,1024]{2,1,0:T(8,128)(2,1)}), bf16[2,1024,1024]{2,1,0:T(8,128)(2,1)}) %all-gather.5.cloned.1.call-update) | async-done | bytes 4194320 | tf_op jit(solution)/shard_map/all_gather | solution.py:88
  192.2 3.2 %slice_bitcast_fusion = (bf16[128,8,8,128]{3,1,2,0:T(8,128)(2,1)S(1)}, bf16[128,8,8,128]{3,1,2,0:T(8,128)(2,1)S(1)}) fusion(bf16[2,1024,1024]{2,1,0:T(8,128)(2,1)} %all-gather.5.cloned.1.call-done), kind=kLoop, calls=%fused_computation.18 | loop fusion | bytes 8388608
  195.4 0.6 copy.83
  196.1 1.3 fusion.16
  197.3 0.0 slice-start.2
  197.4 0.7 bitcast_reduce_fusion
  198.1 0.0 slice-start.3
  198.1 1.9 fusion.3
  200.0 1.0 slice-done.3
  201.0 2.0 fusion.2
  203.0 0.6 copy.84
  203.7 3.3 %fusion.21 = f32[8,32,8,128]{3,1,2,0:T(8,128)S(1)} fusion(bf16[1024,8,128]{2,1,0:T(8,128)(2,1)S(1)} %bitcast.143, f32[8,32,8]{1,0,2:T(8,128)S(1)} %copy.67, f32[8,32,8]{1,0,2:T(8,128)S(1)} %copy.63, f32[8,1024,256]{1,2,0:S(1)} %fusion.16), kind=kOutput, calls=%fused_computation.31 | convolution fusion | flops 545259520 | bytes 11550720 | tf_op jit(solution)/shard_map/rqhc,chd->rqhd/dot_general | solution.py:156
  207.0 2.3 %fusion.29 = bf16[8,32,8,128]{3,1,2,0:T(8,128)(2,1)S(1)} fusion(f32[8,32,8,128]{3,1,2,0:T(8,128)S(1)} %fusion.21, f32[8,32,8,8,32]{1,4,3,2,0:T(8,128)S(1)} %bitcast.135, f32[8,32,8]{1,2,0:T(8,128)S(1)} %copy_add_fusion, f32[8,32,8]{1,2,0:T(8,128)S(1)} %copy_maximum_fusion, bf16[8,8,32,8,128]{4,3,2,1,0:T(8,128)(2,1)S(1)} %bitcast.142), kind=kOutput, calls=%fused_computation.33 | convolution fusion | flops 136314880 | bytes 7880704 | tf_op jit(solution)/shard_map/rqhkw,rkwhd->rqhd/dot_general | solution.py:153
  209.3 0.2 copy.70
  209.5 0.0 copy-start.2
  209.5 0.0 copy-start.1
  209.5 4.5 %convolution_convert_fusion = bf16[256,2048]{1,0:T(8,128)(2,1)} fusion(bf16[1024,2048]{1,0:T(8,128)(2,1)} %param.24, bf16[32,8,8,128]{3,2,1,0:T(8,128)(2,1)S(1)} %bitcast.149), kind=kOutput, calls=%fused_computation.17 | convolution fusion | flops 1074266112 | bytes 5767168 | tf_op jit(solution)/shard_map/dot_general | solution.py:161
  214.0 0.0 reduce-scatter.2.cloned.1.call-update
  214.0 7.1 %reduce-scatter.2.cloned.1.call-done = bf16[128,2048]{1,0:T(8,128)(2,1)} async-done(((bf16[256,2048]{1,0:T(8,128)(2,1)}), bf16[128,2048]{1,0:T(8,128)(2,1)}) %reduce-scatter.2.cloned.1.call-update) | async-done | bytes 524304 | tf_op jit(solution)/shard_map/reduce_scatter | solution.py:160
  221.2 2.0 fusion.40
  (37 shorter events, 0.2 us)
Async XLA Ops:
  6.5 1.0 copy-start
  6.5 93.9 %copy-start.7 = (f32[2048]{0:T(1024)S(1)}, f32[2048]{0:T(1024)}, u32[]{:S(2)}) copy-start(f32[2048]{0:T(1024)} %param.17) | copy-start | bytes 24580
  6.5 94.0 %copy-start.6 = (bf16[64,2048]{1,0:T(8,128)(2,1)S(1)}, bf16[64,2048]{1,0:T(8,128)(2,1)}, u32[]{:S(2)}) copy-start(bf16[64,2048]{1,0:T(8,128)(2,1)} %param.14) | copy-start | bytes 786436
  6.5 112.3 %all-gather.3.cloned.1.call-start = ((), (), s32[]{:S(2)}) async-start(), calls=%async_computation.1 | async-start | bytes 1572864 | tf_op jit(solution)/shard_map/all_gather | solution.py:87
  95.6 96.7 %all-gather.5.cloned.1.call-start = ((), (), s32[]{:S(2)}) async-start(), calls=%async_computation.2 | async-start | bytes 4456448 | tf_op jit(solution)/shard_map/all_gather | solution.py:88
  95.6 4.9 %copy-start.3 = (bf16[2048,1024]{1,0:T(8,128)(2,1)S(1)}, bf16[2048,1024]{1,0:T(8,128)(2,1)}, u32[]{:S(2)}) copy-start(bf16[2048,1024]{1,0:T(8,128)(2,1)} %param.23) | copy-start | bytes 12582916
  96.9 5.4 %copy-start.8 = (f32[16,15,31]{2,0,1:T(8,128)S(1)}, f32[16,15,31]{2,0,1:T(8,128)}, u32[]{:S(2)}) copy-start(f32[16,15,31]{2,0,1:T(8,128)} %param.25) | copy-start | bytes 89284
  102.2 119.0 %reduce-scatter.2.cloned.1.call-start = ((), (), s32[]{:S(2)}) async-start(), calls=%async_computation.3 | async-start | bytes 1572864 | tf_op jit(solution)/shard_map/reduce_scatter | solution.py:160
  118.8 3.9 %copy-start.4 = (bf16[2048,1024]{1,0:T(8,128)(2,1)S(1)}, bf16[2048,1024]{1,0:T(8,128)(2,1)}, u32[]{:S(2)}) copy-start(bf16[2048,1024]{1,0:T(8,128)(2,1)} %param.22) | copy-start | bytes 12582916
  118.8 4.0 %copy-start.10 = (bf16[256,2048]{1,0:T(8,128)(2,1)S(1)}, bf16[256,2048]{1,0:T(8,128)(2,1)}, u32[]{:S(2)}) copy-start(bf16[256,2048]{1,0:T(8,128)(2,1)} %all-gather.3.cloned.1.call-done) | copy-start | bytes 3145732
  122.9 4.0 %copy-start.9 = (bf16[2048,1024]{1,0:T(8,128)(2,1)S(1)}, bf16[2048,1024]{1,0:T(8,128)(2,1)}, u32[]{:S(2)}) copy-start(bf16[2048,1024]{1,0:T(8,128)(2,1)} %param.21) | copy-start | bytes 12582916
  124.2 31.9 %collective-permute-start = (bf16[2,4,32,1024]{3,2,0,1:T(8,128)(2,1)S(1)}, bf16[2,4,32,1024]{3,2,0,1:T(8,128)(2,1)S(1)}, u32[]{:S(2)}, u32[]{:S(2)}) collective-permute-start(bf16[2,4,32,1024]{3,2,0,1:T(8,128)(2,1)S(1)} %get-tuple-element.9), channel_id=1, source_target_pairs={{0,2},{2,4},{4,6},{6,8},{8,10},{10,12},{12,14},{14,16},{16,18},{18... | collective-permute-start | bytes 1572872 | tf_op jit(solution)/shard_map/ppermute | solution.py:24
  125.6 30.6 %collective-permute-start.1 = (bf16[2,4,32,1024]{3,2,0,1:T(8,128)(2,1)S(1)}, bf16[2,4,32,1024]{3,2,0,1:T(8,128)(2,1)S(1)}, u32[]{:S(2)}, u32[]{:S(2)}) collective-permute-start(bf16[2,4,32,1024]{3,2,0,1:T(8,128)(2,1)S(1)} %get-tuple-element.10), channel_id=1, source_target_pairs={{2,0},{4,2},{6,4},{8,6},{10,8},{12,10},{14,12},{16,14},{18,16},{20... | collective-permute-start | bytes 1572872 | tf_op jit(solution)/shard_map/ppermute | solution.py:26
  165.8 4.3 %slice-start = ((s8[8388608]{0:T(1024)(128)(4,1)}), s8[4194304]{0:T(1024)(128)(4,1)S(1)}, s32[]{:S(2)}) async-start(s8[8388608]{0:T(1024)(128)(4,1)} %bitcast.132), calls=%async_computation.4 | async-start | bytes 8388608
  166.9 3.1 %slice-start.1 = ((s8[8388608]{0:T(1024)(128)(4,1)}), s8[4194304]{0:T(1024)(128)(4,1)S(1)}, s32[]{:S(2)}) async-start(s8[8388608]{0:T(1024)(128)(4,1)} %bitcast.132), calls=%async_computation.5 | async-start | bytes 8388608
  197.3 2.6 %slice-start.2 = ((s8[8388608]{0:T(1024)(128)(4,1)}), s8[4194304]{0:T(1024)(128)(4,1)S(1)}, s32[]{:S(2)}) async-start(s8[8388608]{0:T(1024)(128)(4,1)} %bitcast.134), calls=%async_computation.6 | async-start | bytes 8388608
  198.1 2.9 %slice-start.3 = ((s8[8388608]{0:T(1024)(128)(4,1)}), s8[4194304]{0:T(1024)(128)(4,1)S(1)}, s32[]{:S(2)}) async-start(s8[8388608]{0:T(1024)(128)(4,1)} %bitcast.134), calls=%async_computation.7 | async-start | bytes 8388608
  203.7 3.3 %copy-start.5 = (bf16[256,8,8,128]{3,2,1,0:T(8,128)(2,1)S(1)}, bf16[256,8,8,128]{3,2,1,0:T(8,128)(2,1)}, u32[]{:S(2)}) copy-start(bf16[256,8,8,128]{3,2,1,0:T(8,128)(2,1)} %copy.80) | copy-start | bytes 12582916
  209.5 11.7 %copy-start.2 = (bf16[128,2048]{1,0:T(8,128)(2,1)S(1)}, bf16[128,2048]{1,0:T(8,128)(2,1)}, u32[]{:S(2)}) copy-start(bf16[128,2048]{1,0:T(8,128)(2,1)} %param.13) | copy-start | bytes 1572868
  209.5 13.6 %copy-start.1 = (bf16[128,1024]{1,0:T(8,128)(2,1)S(1)}, bf16[128,1024]{1,0:T(8,128)(2,1)}, u32[]{:S(2)}) copy-start(bf16[128,1024]{1,0:T(8,128)(2,1)} %param.18) | copy-start | bytes 786436
Sparse Core Ops, SparseCore 0:
  95.7 5.1 all-gather.2
  103.6 88.6 all-gather.4
  214.2 6.9 reduce-scatter.1
